TPU v7x, 128 devices: a whole 4x4x4 slice. The times are simulated.
128 devices in a mesh: tp: 16 (over z, y), dp: 8 (over x, core).
Axes of the slice: x: 4, y: 4, z: 4, core: 2. Of those that a mesh axis runs over, the one named last changes fastest.
Arguments:
- tokens: bfloat16 [256, 4096], P('dp', 'tp'), may hold values from -6 to 6
- lengths: int32 [256], P('dp'), may hold values from 1 to 96, 6144 in all
- norm_gain: float32 [2, 4096], replicated, may hold values from 0.1 to 1.9
- w_recept: bfloat16 [2, 4096, 4096], P(None, None, ('tp', 'dp')), may hold values from -0.09375 to 0.09375
- w_key: bfloat16 [2, 4096, 4096], P(None, None, ('tp', 'dp')), may hold values from -0.09375 to 0.09375
- w_value: bfloat16 [2, 4096, 4096], P(None, None, ('tp', 'dp')), may hold values from -0.09375 to 0.09375
- w_decay: bfloat16 [2, 4096, 4096], P(None, None, ('tp', 'dp')), may hold values from -0.09375 to 0.09375
- w_rate: bfloat16 [2, 4096, 4096], P(None, None, ('tp', 'dp')), may hold values from -0.09375 to 0.09375
- w_gate: bfloat16 [2, 4096, 4096], P(None, None, ('tp', 'dp')), may hold values from -0.09375 to 0.09375
- w_out: bfloat16 [2, 4096, 4096], P(None, None, ('tp', 'dp')), may hold values from -0.09375 to 0.09375
- decay_base: float32 [2, 4096], P(None, 'tp'), may hold values from -3 to 1
- rate_base: float32 [2, 4096], P(None, 'tp'), may hold values from -3 to 3
- group_gain: float32 [2, 4096], P(None, 'tp'), may hold values from 0.1 to 1.9
- state: float32 [2, 256, 64, 64, 64], P(None, 'dp', 'tp'), may hold values from -6 to 6
Outputs:
- mixed: bfloat16 [256, 4096], P('dp', 'tp')
- new_state: float32 [2, 256, 64, 64, 64], P(None, 'dp', 'tp')
Inputs may be any that keep to these rules, and one draw needn't show every extreme that they name: Each sequence's live length lies between 1 and 96, some sequences reach 96, and the lengths sum to 6144.
All inputs are finite; a program needn't handle non-finite values.
Results may differ from a plain program's by a relative error of at most 0.025.
Values may be sent and summed in bfloat16 or wider, within the bound.
No kernel may reach another device: no remote copies, remote signals or barrier semaphores. Data moves between devices by JAX's collectives and lax.ppermute only.
A program may use at most 128 MiB of HBM per device.

v0:
```python
import jax
import jax.numpy as jnp
from jax import lax
from jax.sharding import Mesh
from jax.sharding import PartitionSpec as P

STEP = 16
TP = ("tp_0", "tp_1")
TP_DP = ("tp_0", "tp_1", "dp")


RMS_EPS = 1e-06
GROUP_EPS = 0.00064


def gather_axes(value, axes, dim):
    if not axes:
        return value
    nearer = lax.all_gather(value, axes[-1], axis=dim, tiled=True)
    return gather_axes(nearer, axes[:-1], dim)


def shortened(value):
    def short(part):
        return part.astype(jnp.bfloat16) if part.dtype == jnp.float32 else part

    return jax.tree.map(short, value)


def over_axes(value, axes, dim, absorb, carry):
    everything = jax.tree.map(lambda part: gather_axes(part, axes, dim), value)
    return absorb(carry, everything, jnp.int32(0))


def recur(state_old, recept, key_vec, value_vec, decay_rate, learn_rate, active, head_size):
    split = (recept.shape[0], -1, head_size)
    recept_h = recept.reshape(split)
    key_h = key_vec.reshape(split)
    value_h = value_vec.reshape(split)
    decay_h = decay_rate.reshape(split)
    rate_h = learn_rate.reshape(split)
    key_len = jnp.sqrt(jnp.sum(key_h * key_h, axis=-1, keepdims=True))
    key_unit = key_h / jnp.maximum(key_len, 1e-12)
    state_a = jnp.einsum("bhij,bhj->bhi", state_old, -key_unit, precision=lax.Precision.DEFAULT)
    updated = (
        state_old * decay_h[:, :, None, :]
        + state_a[:, :, :, None] * (key_unit * rate_h)[:, :, None, :]
        + value_h[:, :, :, None] * (key_h * rate_h)[:, :, None, :]
    )
    updated = jnp.where(active[:, None, None, None], updated, state_old)
    readout = jnp.einsum("bhij,bhj->bhi", updated, recept_h, precision=lax.Precision.DEFAULT)
    centre = jnp.mean(readout, axis=-1, keepdims=True)
    spread = jnp.mean(jnp.square(readout - centre), axis=-1, keepdims=True)
    normal_out = ((readout - centre) * lax.rsqrt(spread + GROUP_EPS)).reshape(recept.shape[0], -1)
    return (updated, normal_out)


def local(
    tokens,
    lengths,
    norm_gain,
    w_recept,
    w_key,
    w_value,
    w_decay,
    w_rate,
    w_gate,
    w_out,
    decay_base,
    rate_base,
    group_gain,
    state,
):
    slim = w_recept.shape[2]
    head_size = state.shape[-1]
    active = lengths > STEP
    current = tokens
    updated_states = []
    for layer_idx in range(2):
        joined = jnp.concatenate(
            [
                w_recept[layer_idx],
                w_key[layer_idx],
                w_value[layer_idx],
                w_decay[layer_idx],
                w_rate[layer_idx],
                w_gate[layer_idx],
            ],
            axis=1,
        )
        batch_raw = lax.all_gather(current, "dp", axis=0, tiled=True)
        every_feature = gather_axes(batch_raw, TP, 1)
        values = every_feature.astype(jnp.float32)
        factor = lax.rsqrt(jnp.mean(values * values, axis=1, keepdims=True) + RMS_EPS)
        normed = (values * factor * norm_gain[layer_idx]).astype(jnp.bfloat16)
        projected = jnp.dot(normed, joined, preferred_element_type=jnp.float32)
        pieces = [
            projected[:, idx * slim : (idx + 1) * slim].astype(jnp.bfloat16) for idx in range(6)
        ]
        arrived = (
            lax.all_to_all(shortened(pieces[0]), "dp", split_axis=0, concat_axis=1, tiled=True),
            lax.all_to_all(shortened(pieces[1]), "dp", split_axis=0, concat_axis=1, tiled=True),
            lax.all_to_all(shortened(pieces[2]), "dp", split_axis=0, concat_axis=1, tiled=True),
            lax.all_to_all(shortened(pieces[3]), "dp", split_axis=0, concat_axis=1, tiled=True),
            lax.all_to_all(shortened(pieces[4]), "dp", split_axis=0, concat_axis=1, tiled=True),
            lax.all_to_all(shortened(pieces[5]), "dp", split_axis=0, concat_axis=1, tiled=True),
        )
        recept, key_vec, value_vec, decay_pre, rate_pre, gate_pre = [
            item.astype(jnp.float32) for item in arrived
        ]
        decay_rate = jnp.exp(-jnp.exp(-jax.nn.softplus(-(decay_base[layer_idx] + decay_pre)) - 0.5))
        learn_rate = jax.nn.sigmoid(rate_base[layer_idx] + rate_pre)
        gate_open = jax.nn.sigmoid(gate_pre)
        updated, normal_out = recur(
            state[layer_idx], recept, key_vec, value_vec, decay_rate, learn_rate, active, head_size
        )
        updated_states.append(updated)
        mixed_here = jnp.where(
            active[:, None], normal_out * group_gain[layer_idx] * gate_open, 0.0
        ).astype(jnp.bfloat16)
        rows_all = lax.all_gather(mixed_here, "dp", axis=0, tiled=True)
        out_weight = w_out[layer_idx]

        def fold_output(acc_sum, segment, offset):
            weight_rows = lax.dynamic_slice_in_dim(out_weight, offset, segment.shape[1], 0)
            return acc_sum + jnp.dot(segment, weight_rows, preferred_element_type=jnp.float32)

        blank = jnp.zeros((rows_all.shape[0], out_weight.shape[1]), jnp.float32)
        out_cols = over_axes(rows_all, TP, 1, fold_output, blank).astype(jnp.bfloat16)
        current = lax.all_to_all(out_cols, "dp", split_axis=0, concat_axis=1, tiled=True)
    return (current, jnp.stack(updated_states))


def solution(mesh):
    finer = Mesh(mesh.devices.reshape(4, 4, mesh.shape["dp"]), ("tp_0", "tp_1", "dp"))
    in_specs = (
        P("dp", TP),
        P("dp"),
        P(),
        P(None, None, TP_DP),
        P(None, None, TP_DP),
        P(None, None, TP_DP),
        P(None, None, TP_DP),
        P(None, None, TP_DP),
        P(None, None, TP_DP),
        P(None, None, TP_DP),
        P(None, TP),
        P(None, TP),
        P(None, TP),
        P(None, "dp", TP, None, None),
    )
    out_specs = (P("dp", TP), P(None, "dp", TP, None, None))
    return jax.shard_map(local, mesh=finer, in_specs=in_specs, out_specs=out_specs, check_vma=False)
```

profile of v0, /device:TPU:1, one launch (start us, length us, event | category | flops | bytes accessed | tf_op | source)
XLA Modules:
  0.0 408.0 jit_solution(4203968245207242246)
XLA Ops:
  7.3 14.8 %all_gather.36 = bf16[256,256]{1,0:T(8,128)(2,1)S(1)} all-gather(bf16[32,256]{1,0:T(8,128)(2,1)} %param.14), channel_id=1, replica_groups=mesh['tp_0'=4,'tp_1'=4,'dp'=8] {'dp'}, dimensions={0}, use_global_device_ids=true | all-gather | bytes 147456 | tf_op jit(solution)/shard_map/all_gather | solution.py:91
  22.0 11.5 %all_gather.37 = bf16[256,1024]{1,0:T(8,128)(2,1)} all-gather(bf16[256,256]{1,0:T(8,128)(2,1)S(1)} %all_gather.36), channel_id=1, replica_groups=mesh['tp_0'=4,'tp_1'=4,'dp'=8] {'tp_1'}, dimensions={1}, use_global_device_ids=true | all-gather | bytes 655360 | tf_op jit(solution)/shard_map/all_gather | solution.py:19
  33.6 0.9 fusion.74
  34.5 1.8 bitcast_dynamic-update-slice_fusion.11
  36.2 1.8 bitcast_dynamic-update-slice_fusion.10
  38.0 1.8 bitcast_dynamic-update-slice_fusion.9
  39.8 0.7 bitcast_dynamic-update-slice_fusion.8
  40.5 0.7 bitcast_dynamic-update-slice_fusion.7
  41.3 0.7 bitcast_dynamic-update-slice_fusion.6
  42.0 25.9 %all-gather.5.cloned.1.call-done = bf16[256,4096]{1,0:T(8,128)(2,1)} async-done(((bf16[256,1024]{1,0:T(8,128)(2,1)}), bf16[256,4096]{1,0:T(8,128)(2,1)}) %all-gather.5.cloned.1.call-update) | async-done | bytes 2097168 | tf_op jit(solution)/shard_map/all_gather | solution.py:19
  67.9 2.1 fusion
  70.0 2.5 fusion.44
  73.4 5.2 %all-to-all-start = ((bf16[8,2,512]{2,1,0:T(2,128)(2,1)}), bf16[8,2,512]{2,1,0:T(2,128)(2,1)S(1)}, u32[]{:S(2)}, u32[]{:S(2)}) async-start(bf16[8,2,512]{2,1,0:T(2,128)(2,1)} %reshape.354), calls=%async_computation | async-start | bytes 32768 | tf_op jit(solution)/shard_map/all_to_all | solution.py:104
  78.9 0.7 reshape.344
  79.7 0.7 reshape.346
  80.5 0.7 reshape.352
  81.4 0.7 reshape.350
  83.2 4.6 %all-to-all-start.5 = ((bf16[8,2,512]{2,1,0:T(2,128)(2,1)}), bf16[8,2,512]{2,1,0:T(2,128)(2,1)S(1)}, u32[]{:S(2)}, u32[]{:S(2)}) async-start(bf16[8,2,512]{2,1,0:T(2,128)(2,1)} %reshape.344), calls=%async_computation.5 | async-start | bytes 32768 | tf_op jit(solution)/shard_map/all_to_all | solution.py:106
  87.9 4.5 %all-to-all-done.5 = bf16[8,2,512]{2,1,0:T(2,128)(2,1)S(1)} async-done(((bf16[8,2,512]{2,1,0:T(2,128)(2,1)}), bf16[8,2,512]{2,1,0:T(2,128)(2,1)S(1)}, u32[]{:S(2)}, u32[]{:S(2)}) %all-to-all-start.5) | async-done | bytes 16416 | tf_op jit(solution)/shard_map/all_to_all | solution.py:106
  92.4 3.9 all-to-all-start.3
  96.5 4.5 %all-to-all-done.3 = bf16[8,2,512]{2,1,0:T(2,128)(2,1)S(1)} async-done(((bf16[8,2,512]{2,1,0:T(2,128)(2,1)}), bf16[8,2,512]{2,1,0:T(2,128)(2,1)S(1)}, u32[]{:S(2)}, u32[]{:S(2)}) %all-to-all-start.3) | async-done | bytes 16416 | tf_op jit(solution)/shard_map/all_to_all | solution.py:103
  101.0 3.9 all-to-all-start.1
  105.1 4.5 %all-to-all-done.1 = bf16[8,2,512]{2,1,0:T(2,128)(2,1)S(1)} async-done(((bf16[8,2,512]{2,1,0:T(2,128)(2,1)}), bf16[8,2,512]{2,1,0:T(2,128)(2,1)S(1)}, u32[]{:S(2)}, u32[]{:S(2)}) %all-to-all-start.1) | async-done | bytes 16416 | tf_op jit(solution)/shard_map/all_to_all | solution.py:102
  109.6 3.9 all-to-all-start.4
  113.7 4.5 %all-to-all-done.4 = bf16[8,2,512]{2,1,0:T(2,128)(2,1)S(1)} async-done(((bf16[8,2,512]{2,1,0:T(2,128)(2,1)}), bf16[8,2,512]{2,1,0:T(2,128)(2,1)S(1)}, u32[]{:S(2)}, u32[]{:S(2)}) %all-to-all-start.4) | async-done | bytes 16416 | tf_op jit(solution)/shard_map/all_to_all | solution.py:101
  118.2 3.9 all-to-all-start.2
  123.1 3.8 all-to-all-done.2
  127.7 3.4 fusion.6
  131.1 4.2 %fusion.10 = f32[32,4,1,64]{3,2,1,0:T(1,128)S(1)} fusion(bf16[32,4,64,1]{2,3,1,0:T(2,128)(2,1)S(1)} %reshape.319, f32[2,32,4,64,64]{4,3,2,1,0:T(8,128)} %param.27, f32[32,4,64]{2,1,0:T(4,128)S(1)} %get-tuple-element.29, f32[32,4,64]{2,1,0:T(4,128)S(1)} %reshape.301, f32[32,4,64]{2,1,0:T(4,128)S(1)} %get-tuple-element.28, f32[32,4,64]{2,1,0:T(4,128)S(1)} %bitcast.139, ...), kind=kOutput, calls=%fused_computation.17 | convolution fusion | flops 4194304 | bytes 4407328 | tf_op jit(solution)/shard_map/bhij,bhj->bhi/dot_general | solution.py:51
  136.0 13.3 %all_gather.39 = bf16[256,256]{1,0:T(8,128)(2,1)S(1)} all-gather(bf16[32,256]{1,0:T(8,128)(2,1)S(1)} %select_convert_fusion.1), channel_id=1, replica_groups=mesh['tp_0'=4,'tp_1'=4,'dp'=8] {'dp'}, dimensions={0}, use_global_device_ids=true | all-gather | bytes 147456 | tf_op jit(solution)/shard_map/all_gather | solution.py:121
  149.2 11.3 %all_gather.40 = bf16[256,1024]{1,0:T(8,128)(2,1)} all-gather(bf16[256,256]{1,0:T(8,128)(2,1)S(1)} %all_gather.39), channel_id=1, replica_groups=mesh['tp_0'=4,'tp_1'=4,'dp'=8] {'tp_1'}, dimensions={1}, use_global_device_ids=true | all-gather | bytes 655360 | tf_op jit(solution)/shard_map/all_gather | solution.py:19
  160.7 30.8 %all-gather.7.cloned.1.call-done = bf16[256,4096]{1,0:T(8,128)(2,1)} async-done(((bf16[256,1024]{1,0:T(8,128)(2,1)}), bf16[256,4096]{1,0:T(8,128)(2,1)}) %all-gather.7.cloned.1.call-update) | async-done | bytes 2097168 | tf_op jit(solution)/shard_map/all_gather | solution.py:19
  191.5 2.3 convolution_convert_fusion.1
  194.1 9.6 %all_to_all.200 = bf16[8,2,512]{2,1,0:T(2,128)(2,1)S(1)} all-to-all(bf16[8,2,512]{2,1,0:T(2,128)(2,1)S(1)} %reshape.356), channel_id=1, replica_groups=mesh['tp_0'=4,'tp_1'=4,'dp'=8] {'dp'}, dimensions={0} | all-to-all | bytes 32768 | tf_op jit(solution)/shard_map/all_to_all | solution.py:130
  203.9 13.3 %all_gather.42 = bf16[256,256]{1,0:T(8,128)(2,1)S(1)} all-gather(bf16[32,256]{1,0:T(8,128)(2,1)S(1)} %all_to_all.168), channel_id=1, replica_groups=mesh['tp_0'=4,'tp_1'=4,'dp'=8] {'dp'}, dimensions={0}, use_global_device_ids=true | all-gather | bytes 147456 | tf_op jit(solution)/shard_map/all_gather | solution.py:91
  217.2 11.3 %all_gather.43 = bf16[256,1024]{1,0:T(8,128)(2,1)} all-gather(bf16[256,256]{1,0:T(8,128)(2,1)S(1)} %all_gather.42), channel_id=1, replica_groups=mesh['tp_0'=4,'tp_1'=4,'dp'=8] {'tp_1'}, dimensions={1}, use_global_device_ids=true | all-gather | bytes 655360 | tf_op jit(solution)/shard_map/all_gather | solution.py:19
  228.6 30.9 %all-gather.9.cloned.1.call-done = bf16[256,4096]{1,0:T(8,128)(2,1)} async-done(((bf16[256,1024]{1,0:T(8,128)(2,1)}), bf16[256,4096]{1,0:T(8,128)(2,1)}) %all-gather.9.cloned.1.call-update) | async-done | bytes 2097168 | tf_op jit(solution)/shard_map/all_gather | solution.py:19
  259.5 2.1 fusion.3
  261.6 3.0 fusion.47
  265.4 5.2 %all-to-all-start.7 = ((bf16[8,2,512]{2,1,0:T(2,128)(2,1)}), bf16[8,2,512]{2,1,0:T(2,128)(2,1)S(1)}, u32[]{:S(2)}, u32[]{:S(2)}) async-start(bf16[8,2,512]{2,1,0:T(2,128)(2,1)} %reshape.368), calls=%async_computation.7 | async-start | bytes 32768 | tf_op jit(solution)/shard_map/all_to_all | solution.py:104
  270.9 0.7 reshape.358
  271.7 0.7 reshape.360
  272.6 0.7 reshape.366
  273.4 0.7 reshape.364
  274.3 0.7 reshape.362
  275.3 4.5 %all-to-all-start.12 = ((bf16[8,2,512]{2,1,0:T(2,128)(2,1)}), bf16[8,2,512]{2,1,0:T(2,128)(2,1)S(1)}, u32[]{:S(2)}, u32[]{:S(2)}) async-start(bf16[8,2,512]{2,1,0:T(2,128)(2,1)} %reshape.358), calls=%async_computation.12 | async-start | bytes 32768 | tf_op jit(solution)/shard_map/all_to_all | solution.py:106
  279.9 4.5 %all-to-all-done.12 = bf16[8,2,512]{2,1,0:T(2,128)(2,1)S(1)} async-done(((bf16[8,2,512]{2,1,0:T(2,128)(2,1)}), bf16[8,2,512]{2,1,0:T(2,128)(2,1)S(1)}, u32[]{:S(2)}, u32[]{:S(2)}) %all-to-all-start.12) | async-done | bytes 16416 | tf_op jit(solution)/shard_map/all_to_all | solution.py:106
  284.4 3.9 all-to-all-start.10
  288.5 4.5 %all-to-all-done.10 = bf16[8,2,512]{2,1,0:T(2,128)(2,1)S(1)} async-done(((bf16[8,2,512]{2,1,0:T(2,128)(2,1)}), bf16[8,2,512]{2,1,0:T(2,128)(2,1)S(1)}, u32[]{:S(2)}, u32[]{:S(2)}) %all-to-all-start.10) | async-done | bytes 16416 | tf_op jit(solution)/shard_map/all_to_all | solution.py:103
  293.1 3.9 all-to-all-start.8
  297.1 4.5 %all-to-all-done.8 = bf16[8,2,512]{2,1,0:T(2,128)(2,1)S(1)} async-done(((bf16[8,2,512]{2,1,0:T(2,128)(2,1)}), bf16[8,2,512]{2,1,0:T(2,128)(2,1)S(1)}, u32[]{:S(2)}, u32[]{:S(2)}) %all-to-all-start.8) | async-done | bytes 16416 | tf_op jit(solution)/shard_map/all_to_all | solution.py:102
  301.7 4.0 all-to-all-start.11
  305.7 4.5 %all-to-all-done.11 = bf16[8,2,512]{2,1,0:T(2,128)(2,1)S(1)} async-done(((bf16[8,2,512]{2,1,0:T(2,128)(2,1)}), bf16[8,2,512]{2,1,0:T(2,128)(2,1)S(1)}, u32[]{:S(2)}, u32[]{:S(2)}) %all-to-all-start.11) | async-done | bytes 16416 | tf_op jit(solution)/shard_map/all_to_all | solution.py:101
  310.3 3.9 all-to-all-start.9
  315.1 3.8 all-to-all-done.9
  319.6 3.4 fusion.11
  323.1 4.2 %fusion.15 = f32[32,4,1,64]{3,2,1,0:T(1,128)S(1)} fusion(bf16[32,4,64,1]{2,3,1,0:T(2,128)(2,1)S(1)} %reshape.321, f32[2,32,4,64,64]{4,3,2,1,0:T(8,128)} %param.27, f32[32,4,64]{2,1,0:T(4,128)S(1)} %get-tuple-element.27, f32[32,4,64]{2,1,0:T(4,128)S(1)} %reshape.307, f32[32,4,64]{2,1,0:T(4,128)S(1)} %get-tuple-element.26, f32[32,4,64]{2,1,0:T(4,128)S(1)} %bitcast.141, ...), kind=kOutput, calls=%fused_computation.24 | convolution fusion | flops 4194304 | bytes 4407328 | tf_op jit(solution)/shard_map/bhij,bhj->bhi/dot_general | solution.py:51
  328.0 13.3 %all_gather.45 = bf16[256,256]{1,0:T(8,128)(2,1)S(1)} all-gather(bf16[32,256]{1,0:T(8,128)(2,1)S(1)} %select_convert_fusion), channel_id=1, replica_groups=mesh['tp_0'=4,'tp_1'=4,'dp'=8] {'dp'}, dimensions={0}, use_global_device_ids=true | all-gather | bytes 147456 | tf_op jit(solution)/shard_map/all_gather | solution.py:121
  341.2 11.3 %all_gather.46 = bf16[256,1024]{1,0:T(8,128)(2,1)} all-gather(bf16[256,256]{1,0:T(8,128)(2,1)S(1)} %all_gather.45), channel_id=1, replica_groups=mesh['tp_0'=4,'tp_1'=4,'dp'=8] {'tp_1'}, dimensions={1}, use_global_device_ids=true | all-gather | bytes 655360 | tf_op jit(solution)/shard_map/all_gather | solution.py:19
  352.6 10.6 %add_select_fusion.1 = (f32[1,32,4,64,64]{4,3,2,1,0:T(8,128)}, f32[1,32,4,64,64]{4,3,2,1,0:T(8,128)}) fusion(f32[2,32,4,64,64]{4,3,2,1,0:T(8,128)} %param.27, f32[32,4,64]{2,1,0:T(4,128)S(1)} %get-tuple-element.29, f32[32,4,64]{2,1,0:T(4,128)S(1)} %reshape.301, f32[32,4,64]{2,1,0:T(4,128)S(1)} %get-tuple-element.28, f32[32,4,64]{2,1,0:T(4,128)S(1)} %bitcast.140, ...), kind=kLoop, calls=%fused_computation.26 | loop fusion | flops 6291456 | bytes 8716320 | tf_op jit(solution)/shard_map/jit(_where)/select_n | solution.py:50
  363.2 20.3 %all-gather.11.cloned.1.call-done = bf16[256,4096]{1,0:T(8,128)(2,1)} async-done(((bf16[256,1024]{1,0:T(8,128)(2,1)}), bf16[256,4096]{1,0:T(8,128)(2,1)}) %all-gather.11.cloned.1.call-update) | async-done | bytes 2097168 | tf_op jit(solution)/shard_map/all_gather | solution.py:19
  383.5 2.3 convolution_convert_fusion
  386.7 5.2 %all-to-all-start.13 = ((bf16[8,2,512]{2,1,0:T(2,128)(2,1)}), bf16[8,2,512]{2,1,0:T(2,128)(2,1)S(1)}, u32[]{:S(2)}, u32[]{:S(2)}) async-start(bf16[8,2,512]{2,1,0:T(2,128)(2,1)} %reshape.370), calls=%async_computation.13 | async-start | bytes 32768 | tf_op jit(solution)/shard_map/all_to_all | solution.py:130
  391.9 8.8 %pad_maximum_fusion = f32[2,32,4,64,64]{4,3,2,1,0:T(8,128)} fusion(f32[1,32,4,64,64]{4,3,2,1,0:T(8,128)} %get-tuple-element.13, f32[1,32,4,64,64]{4,3,2,1,0:T(8,128)} %get-tuple-element.12), kind=kLoop, calls=%fused_computation | loop fusion | flops 1048576 | bytes 8388608 | tf_op jit(solution)/shard_map/stack | solution.py:131
  (135 shorter events, 12.4 us)
Async XLA Ops:
  7.2 32.6 %copy-start.7 = (s32[32]{0:T(128)S(1)}, s32[32]{0:T(128)}, u32[]{:S(2)}) copy-start(s32[32]{0:T(128)} %param.15) | copy-start | bytes 388
  7.2 32.6 %copy-start.4 = (f32[2,256]{1,0:T(2,128)S(1)}, f32[2,256]{1,0:T(2,128)}, u32[]{:S(2)}) copy-start(f32[2,256]{1,0:T(2,128)} %param.26) | copy-start | bytes 6148
  7.2 32.6 %copy-start.1 = (bf16[2,4096,32]{1,2,0:T(8,128)(2,1)S(1)}, bf16[2,4096,32]{1,2,0:T(8,128)(2,1)}, u32[]{:S(2)}) copy-start(bf16[2,4096,32]{1,2,0:T(8,128)(2,1)} %param.20) | copy-start | bytes 1572868
  7.2 33.3 %copy-start.2 = (bf16[2,4096,32]{1,2,0:T(8,128)(2,1)S(1)}, bf16[2,4096,32]{1,2,0:T(8,128)(2,1)}, u32[]{:S(2)}) copy-start(bf16[2,4096,32]{1,2,0:T(8,128)(2,1)} %param.21) | copy-start | bytes 1572868
  7.2 34.1 %copy-start.3 = (bf16[2,4096,32]{1,2,0:T(8,128)(2,1)S(1)}, bf16[2,4096,32]{1,2,0:T(8,128)(2,1)}, u32[]{:S(2)}) copy-start(bf16[2,4096,32]{1,2,0:T(8,128)(2,1)} %param.22) | copy-start | bytes 1572868
  7.2 60.7 %all-gather.5.cloned.1.call-start = ((), (), s32[]{:S(2)}) async-start(), calls=%async_computation.14 | async-start | bytes 2621440 | tf_op jit(solution)/shard_map/all_gather | solution.py:19
  42.0 36.5 %copy-start.5 = (f32[2,256]{1,0:T(2,128)S(1)}, f32[2,256]{1,0:T(2,128)}, u32[]{:S(2)}) copy-start(f32[2,256]{1,0:T(2,128)} %param.25) | copy-start | bytes 6148
  42.0 36.5 %copy-start.6 = (f32[2,256]{1,0:T(2,128)S(1)}, f32[2,256]{1,0:T(2,128)}, u32[]{:S(2)}) copy-start(f32[2,256]{1,0:T(2,128)} %param.24) | copy-start | bytes 6148
  73.4 9.8 %all-to-all-start = ((bf16[8,2,512]{2,1,0:T(2,128)(2,1)}), bf16[8,2,512]{2,1,0:T(2,128)(2,1)S(1)}, u32[]{:S(2)}, u32[]{:S(2)}) async-start(bf16[8,2,512]{2,1,0:T(2,128)(2,1)} %reshape.354), calls=%async_computation | async-start | bytes 32768 | tf_op jit(solution)/shard_map/all_to_all | solution.py:104
  83.2 9.2 %all-to-all-start.5 = ((bf16[8,2,512]{2,1,0:T(2,128)(2,1)}), bf16[8,2,512]{2,1,0:T(2,128)(2,1)S(1)}, u32[]{:S(2)}, u32[]{:S(2)}) async-start(bf16[8,2,512]{2,1,0:T(2,128)(2,1)} %reshape.344), calls=%async_computation.5 | async-start | bytes 32768 | tf_op jit(solution)/shard_map/all_to_all | solution.py:106
  92.4 8.6 %all-to-all-start.3 = ((bf16[8,2,512]{2,1,0:T(2,128)(2,1)}), bf16[8,2,512]{2,1,0:T(2,128)(2,1)S(1)}, u32[]{:S(2)}, u32[]{:S(2)}) async-start(bf16[8,2,512]{2,1,0:T(2,128)(2,1)} %reshape.352), calls=%async_computation.3 | async-start | bytes 32768 | tf_op jit(solution)/shard_map/all_to_all | solution.py:103
  101.0 8.6 %all-to-all-start.1 = ((bf16[8,2,512]{2,1,0:T(2,128)(2,1)}), bf16[8,2,512]{2,1,0:T(2,128)(2,1)S(1)}, u32[]{:S(2)}, u32[]{:S(2)}) async-start(bf16[8,2,512]{2,1,0:T(2,128)(2,1)} %reshape.348), calls=%async_computation.1 | async-start | bytes 32768 | tf_op jit(solution)/shard_map/all_to_all | solution.py:102
  109.6 8.6 %all-to-all-start.4 = ((bf16[8,2,512]{2,1,0:T(2,128)(2,1)}), bf16[8,2,512]{2,1,0:T(2,128)(2,1)S(1)}, u32[]{:S(2)}, u32[]{:S(2)}) async-start(bf16[8,2,512]{2,1,0:T(2,128)(2,1)} %reshape.346), calls=%async_computation.4 | async-start | bytes 32768 | tf_op jit(solution)/shard_map/all_to_all | solution.py:101
  118.2 8.6 %all-to-all-start.2 = ((bf16[8,2,512]{2,1,0:T(2,128)(2,1)}), bf16[8,2,512]{2,1,0:T(2,128)(2,1)S(1)}, u32[]{:S(2)}, u32[]{:S(2)}) async-start(bf16[8,2,512]{2,1,0:T(2,128)(2,1)} %reshape.350), calls=%async_computation.2 | async-start | bytes 32768 | tf_op jit(solution)/shard_map/all_to_all | solution.py:105
  122.2 69.3 %all-gather.7.cloned.1.call-start = ((), (), s32[]{:S(2)}) async-start(), calls=%async_computation.15 | async-start | bytes 2621440 | tf_op jit(solution)/shard_map/all_gather | solution.py:19
  131.1 60.4 %copy-start = (bf16[2,4096,32]{1,2,0:T(8,128)(2,1)S(1)}, bf16[2,4096,32]{1,2,0:T(8,128)(2,1)}, u32[]{:S(2)}) copy-start(bf16[2,4096,32]{1,2,0:T(8,128)(2,1)} %param.23) | copy-start | bytes 1572868
  160.6 98.9 %all-gather.9.cloned.1.call-start = ((), (), s32[]{:S(2)}) async-start(), calls=%async_computation.16 | async-start | bytes 2621440 | tf_op jit(solution)/shard_map/all_gather | solution.py:19
  265.4 9.8 %all-to-all-start.7 = ((bf16[8,2,512]{2,1,0:T(2,128)(2,1)}), bf16[8,2,512]{2,1,0:T(2,128)(2,1)S(1)}, u32[]{:S(2)}, u32[]{:S(2)}) async-start(bf16[8,2,512]{2,1,0:T(2,128)(2,1)} %reshape.368), calls=%async_computation.7 | async-start | bytes 32768 | tf_op jit(solution)/shard_map/all_to_all | solution.py:104
  275.3 9.2 %all-to-all-start.12 = ((bf16[8,2,512]{2,1,0:T(2,128)(2,1)}), bf16[8,2,512]{2,1,0:T(2,128)(2,1)S(1)}, u32[]{:S(2)}, u32[]{:S(2)}) async-start(bf16[8,2,512]{2,1,0:T(2,128)(2,1)} %reshape.358), calls=%async_computation.12 | async-start | bytes 32768 | tf_op jit(solution)/shard_map/all_to_all | solution.py:106
  284.4 8.6 %all-to-all-start.10 = ((bf16[8,2,512]{2,1,0:T(2,128)(2,1)}), bf16[8,2,512]{2,1,0:T(2,128)(2,1)S(1)}, u32[]{:S(2)}, u32[]{:S(2)}) async-start(bf16[8,2,512]{2,1,0:T(2,128)(2,1)} %reshape.366), calls=%async_computation.10 | async-start | bytes 32768 | tf_op jit(solution)/shard_map/all_to_all | solution.py:103
  293.1 8.6 %all-to-all-start.8 = ((bf16[8,2,512]{2,1,0:T(2,128)(2,1)}), bf16[8,2,512]{2,1,0:T(2,128)(2,1)S(1)}, u32[]{:S(2)}, u32[]{:S(2)}) async-start(bf16[8,2,512]{2,1,0:T(2,128)(2,1)} %reshape.362), calls=%async_computation.8 | async-start | bytes 32768 | tf_op jit(solution)/shard_map/all_to_all | solution.py:102
  301.7 8.6 %all-to-all-start.11 = ((bf16[8,2,512]{2,1,0:T(2,128)(2,1)}), bf16[8,2,512]{2,1,0:T(2,128)(2,1)S(1)}, u32[]{:S(2)}, u32[]{:S(2)}) async-start(bf16[8,2,512]{2,1,0:T(2,128)(2,1)} %reshape.360), calls=%async_computation.11 | async-start | bytes 32768 | tf_op jit(solution)/shard_map/all_to_all | solution.py:101
  310.3 8.6 %all-to-all-start.9 = ((bf16[8,2,512]{2,1,0:T(2,128)(2,1)}), bf16[8,2,512]{2,1,0:T(2,128)(2,1)S(1)}, u32[]{:S(2)}, u32[]{:S(2)}) async-start(bf16[8,2,512]{2,1,0:T(2,128)(2,1)} %reshape.364), calls=%async_computation.9 | async-start | bytes 32768 | tf_op jit(solution)/shard_map/all_to_all | solution.py:105
  314.2 69.3 %all-gather.11.cloned.1.call-start = ((), (), s32[]{:S(2)}) async-start(), calls=%async_computation.17 | async-start | bytes 2621440 | tf_op jit(solution)/shard_map/all_gather | solution.py:19
  386.7 13.9 %all-to-all-start.13 = ((bf16[8,2,512]{2,1,0:T(2,128)(2,1)}), bf16[8,2,512]{2,1,0:T(2,128)(2,1)S(1)}, u32[]{:S(2)}, u32[]{:S(2)}) async-start(bf16[8,2,512]{2,1,0:T(2,128)(2,1)} %reshape.370), calls=%async_computation.13 | async-start | bytes 32768 | tf_op jit(solution)/shard_map/all_to_all | solution.py:130
Sparse Core Ops, SparseCore 0:
  33.7 34.1 all-gather.4
  160.7 30.7 all-gather.6
  228.7 30.7 all-gather.8
  352.7 30.7 all-gather.10
where the time goes:
time: 410 us; the launch traced here: 408 us
  waiting for transfers between devices  152 us (37%)
  blocking collectives  110 us (27%)
  starting transfers between devices  56.2 us (14%)
  other arithmetic  25.6 us (6%)
  matrix products  25.2 us (6%)
  local copies, waits for them, and re-layouts  24.6 us (6%)
  between operations  14.3 us (3%)
    all_gather x4, waiting for transfers between devices, gather_axes(): nearer = lax.all_gather(value, axes[-1], axis=dim, tiled=True)  108 us
    all_gather x4, blocking collectives, gather_axes(): nearer = lax.all_gather(value, axes[-1], axis=dim, tiled=True)  45.5 us
    all_gather x2, blocking collectives, local(): batch_raw = lax.all_gather(current, 'dp', axis=0, tiled=True)  28.1 us
    all_gather x2, blocking collectives, local(): rows_all = lax.all_gather(mixed_here, 'dp', axis=0, tiled=True)  26.6 us
    unnamed x50, local copies, waits for them, and re-layouts  18.4 us
    select_n x1, other arithmetic, recur(): updated = jnp.where(active[:, None, None, None], updated, state_old)  10.6 us
    all_to_all x2, starting transfers between devices, local(): lax.all_to_all(shortened(pieces[3]), 'dp', split_axis=0, concat_axis=1, t...  10.4 us
    all_to_all x1, blocking collectives, local(): lax.all_to_all(out_cols, 'dp', split_axis=0, concat_axis=1, tiled=True)  9.62 us
  transfers between devices with their start and end apart: 17, of which 16 were waited for; matrix products, arithmetic and copies ran while one was open for 10% of the time, Pallas kernels for 0%

commit v1 on v0

v1 whole, which is shorter than its diff:
```python
import jax
import jax.numpy as jnp
from jax import lax
from jax.sharding import Mesh
from jax.sharding import PartitionSpec as P

STEP = 16
RMS_EPS = 1e-06
GROUP_EPS = 0.00064
TP = ("z", "y")
DP = ("x", "c")
CHIPS = ("z", "y", "x")
PAIR = [(0, 1), (1, 0)]


def spread(value):
    count = lax.axis_size(CHIPS)
    copies = jnp.broadcast_to(value[None], (count,) + value.shape)
    return lax.all_to_all(copies, CHIPS, 0, 0)


def both_cores(own, peer, core):
    first = jnp.where(core == 0, own, peer)
    second = jnp.where(core == 0, peer, own)
    return jnp.concatenate([first, second], axis=-1)


def recur(state_old, recept_h, key_h, value_h, decay_h, rate_h, active):
    key_len = jnp.sqrt(jnp.sum(key_h * key_h, axis=-1, keepdims=True))
    key_unit = key_h / jnp.maximum(key_len, 1e-12)
    state_a = jnp.einsum("bhij,bhj->bhi", state_old, -key_unit, precision=lax.Precision.DEFAULT)
    updated = (
        state_old * decay_h[:, :, None, :]
        + state_a[:, :, :, None] * (key_unit * rate_h)[:, :, None, :]
        + value_h[:, :, :, None] * (key_h * rate_h)[:, :, None, :]
    )
    updated = jnp.where(active[:, None, None, None], updated, state_old)
    readout = jnp.einsum("bhij,bhj->bhi", updated, recept_h, precision=lax.Precision.DEFAULT)
    centre = jnp.mean(readout, axis=-1, keepdims=True)
    spread_ = jnp.mean(jnp.square(readout - centre), axis=-1, keepdims=True)
    return updated, (readout - centre) * lax.rsqrt(spread_ + GROUP_EPS)


def local(
    tokens, lengths, norm_gain, w_recept, w_key, w_value, w_decay, w_rate, w_gate, w_out,
    decay_base, rate_base, group_gain, state,
):
    core = lax.axis_index("c")
    rows, feats = tokens.shape
    heads, head = state.shape[2], state.shape[-1]
    n_x = lax.axis_size("x")
    n_tp = lax.axis_size(TP)
    active = lengths > STEP
    weights = []
    for w in (w_recept, w_key, w_value, w_decay, w_rate, w_gate, w_out):
        own = w.swapaxes(1, 2)
        weights.append((own, lax.ppermute(own, "c", PAIR)))
    updated_states = []
    natural = spread(tokens).reshape(n_tp, n_x, rows, feats).transpose(1, 2, 0, 3)
    natural = natural.reshape(n_x * rows, n_tp * feats)
    for layer in range(2):
        joined = jnp.concatenate([p[layer] for own_peer in weights[:6] for p in own_peer], axis=0)
        values = natural.astype(jnp.float32)
        factor = lax.rsqrt(jnp.mean(values * values, axis=1, keepdims=True) + RMS_EPS)
        normed = (values * factor * norm_gain[layer]).astype(jnp.bfloat16)
        projected = lax.dot_general(
            normed, joined, (((1,), (1,)), ((), ())), preferred_element_type=jnp.float32
        ).astype(jnp.bfloat16)
        arrived = lax.all_to_all(projected.reshape(n_x, rows, -1), "x", 0, 0)
        parts = arrived.reshape(heads, rows, 6, 2, head // 2).astype(jnp.float32)
        recept, key_vec, value_vec, decay_pre, rate_pre, gate_pre = [
            jnp.concatenate(
                [
                    jnp.where(core == 0, parts[:, :, m, 0], parts[:, :, m, 1]),
                    jnp.where(core == 0, parts[:, :, m, 1], parts[:, :, m, 0]),
                ],
                axis=-1,
            ).transpose(1, 0, 2)
            for m in range(6)
        ]
        decay_b = decay_base[layer].reshape(heads, head)
        rate_b = rate_base[layer].reshape(heads, head)
        gain_b = group_gain[layer].reshape(heads, head)
        decay_rate = jnp.exp(-jnp.exp(-jax.nn.softplus(-(decay_b + decay_pre)) - 0.5))
        learn_rate = jax.nn.sigmoid(rate_b + rate_pre)
        gate_open = jax.nn.sigmoid(gate_pre)
        updated, normal_out = recur(
            state[layer], recept, key_vec, value_vec, decay_rate, learn_rate, active
        )
        updated_states.append(updated)
        mixed_here = jnp.where(active[:, None, None], normal_out * gain_b * gate_open, 0.0)
        mixed_here = mixed_here.astype(jnp.bfloat16).reshape(rows, feats)
        mixed_all = spread(mixed_here).reshape(n_tp, n_x, rows, feats).transpose(1, 2, 0, 3)
        mixed_all = mixed_all.reshape(n_x * rows, n_tp * feats)
        own, peer = weights[6]
        out_w = jnp.concatenate([own[layer], peer[layer]], axis=0)
        cols = lax.dot_general(
            out_w, mixed_all, (((1,), (1,)), ((), ())), preferred_element_type=jnp.float32
        ).astype(jnp.bfloat16)
        half = cols.shape[0] // 2
        cols = jnp.where(core == 0, cols, jnp.concatenate([cols[half:], cols[:half]], axis=0))
        if layer == 0:
            natural = spread(cols).reshape(n_tp * feats, n_x * rows).T
        else:
            blocks = cols.reshape(2 * half, n_x, rows).transpose(1, 2, 0)
            back = lax.all_to_all(blocks, "x", 0, 0)
            mixed = back.transpose(1, 0, 2).reshape(rows, feats)
    return mixed, jnp.stack(updated_states)


def solution(mesh):
    finer = Mesh(mesh.devices.reshape(4, 4, mesh.shape["dp"] // 2, 2), ("z", "y", "x", "c"))
    wide = P(None, None, TP + DP)
    in_specs = (
        (P(DP, TP), P(DP), P()) + (wide,) * 7 + (P(None, TP),) * 3 + (P(None, DP, TP, None, None),)
    )
    out_specs = (P(DP, TP), P(None, DP, TP, None, None))
    return jax.shard_map(local, mesh=finer, in_specs=in_specs, out_specs=out_specs, check_vma=False)
```

time: 410 us -> 177 us (0.43)
  waiting for transfers between devices: 152 us -> 36.1 us
  blocking collectives: 110 us -> 24.6 us
  starting transfers between devices: 56.2 us -> 36.5 us
  between operations: 14.3 us -> 1.23 us
  local copies, waits for them, and re-layouts: 24.6 us -> 30.7 us
    all_gather x4 -> x0, waiting for transfers between devices: 108 us -> none  [gather_axes(): nearer = lax.all_gather(value, axes[-1], axis=dim, tiled=True)]
    all_gather x8 -> x0, blocking collectives: 100 us -> none  [the longest x4 45.5 us: gather_axes(): nearer = lax.all_gather(value, axes[-1], axis=dim, tiled=True)]
    all_to_all x13 -> x6, starting transfers between devices: 56.1 us -> 33.4 us  [the longest x3 23.2 us: spread(): return lax.all_to_all(copies, CHIPS, 0, 0)]
    all_to_all x1, blocking collectives: 9.62 us -> 24.6 us  [spread(): return lax.all_to_all(copies, CHIPS, 0, 0)]
    all_to_all x13 -> x6, waiting for transfers between devices: 44.3 us -> 36 us  [the longest x3 27.7 us: spread(): return lax.all_to_all(copies, CHIPS, 0, 0)]
    broadcast_in_dim x0 -> x6, local copies, waits for them, and re-layouts: none -> 4.46 us  [spread(): copies = jnp.broadcast_to(value[None], (count,) + value.shape)]
    unnamed x50 -> x42, local copies, waits for them, and re-layouts: 18.4 us -> 17.5 us
  transfers between devices with their start and end apart: 17 -> 13, of which waited for: 16 -> 5; matrix products, arithmetic and copies ran while one was open for 10% -> 33% of each run, Pallas kernels for 0% -> 0%
where the time goes in v1:
time: 177 us; the launch traced here: 176 us
  starting transfers between devices  36.5 us (21%)
  waiting for transfers between devices  36.1 us (20%)
  local copies, waits for them, and re-layouts  30.7 us (17%)
  blocking collectives  24.6 us (14%)
  other arithmetic  24.4 us (14%)
  matrix products  22.1 us (12%)
    all_to_all x3, waiting for transfers between devices, spread(): return lax.all_to_all(copies, CHIPS, 0, 0)  27.7 us
    all_to_all x1, blocking collectives, spread(): return lax.all_to_all(copies, CHIPS, 0, 0)  24.6 us
    all_to_all x3, starting transfers between devices, spread(): return lax.all_to_all(copies, CHIPS, 0, 0)  23.2 us
    unnamed x42, local copies, waits for them, and re-layouts  17.5 us
    select_n x1, other arithmetic, recur(): updated = jnp.where(active[:, None, None, None], updated, state_old)  10.7 us
    another operation x1, other arithmetic, local(): return (mixed, jnp.stack(updated_states))  8.77 us
    all_to_all x2, waiting for transfers between devices, local(): arrived = lax.all_to_all(projected.reshape(n_x, rows, -1), 'x', 0, 0)  8.39 us
    dot_general x2, matrix products, recur(): jnp.einsum('bhij,bhj->bhi', updated, recept_h, precision=lax.Precision.DE...  8.32 us
  transfers between devices with their start and end apart: 13, of which 5 were waited for; matrix products, arithmetic and copies ran while one was open for 33% of the time, Pallas kernels for 0%

profile of v1, /device:TPU:1, one launch (start us, length us, event | category | flops | bytes accessed | tf_op | source)
XLA Modules:
  0.0 175.7 jit_solution(12496871022072852600)
XLA Ops:
  0.7 1.4 collective-permute-start.1
  2.2 0.4 collective-permute-start.3
  2.7 0.4 collective-permute-start.5
  3.2 1.8 %broadcast_in_dim.41 = bf16[64,32,256]{2,1,0:T(8,128)(2,1)} broadcast(bf16[32,256]{1,0:T(8,128)(2,1)} %param.14), dimensions={1,2} | broadcast | bytes 1064960 | tf_op jit(solution)/shard_map/broadcast_in_dim | solution.py:18
  5.0 11.4 %all-to-all-start = ((bf16[64,32,256]{2,1,0:T(8,128)(2,1)}), bf16[64,32,256]{2,1,0:T(8,128)(2,1)S(1)}, u32[]{:S(2)}, u32[]{:S(2)}) async-start(bf16[64,32,256]{2,1,0:T(8,128)(2,1)} %broadcast_in_dim.41), calls=%async_computation | async-start | bytes 2097152 | tf_op jit(solution)/shard_map/all_to_all | solution.py:19
  16.4 0.8 fusion.67
  17.4 0.5 collective-permute-start.6
  17.9 1.9 %fusion.66 = (bf16[384,4096]{1,0:T(8,128)(2,1)}, bf16[384,4096]{1,0:T(8,128)(2,1)}) fusion(bf16[384,4096]{1,0:T(8,128)(2,1)} %get-tuple-element.68, bf16[2,32,4096]{2,1,0:T(8,128)(2,1)} %collective-permute-done.1, bf16[384,4096]{1,0:T(8,128)(2,1)} %get-tuple-element.69), kind=kLoop, calls=%fused_computation.103 | loop fusion | bytes 1048576
  19.7 0.8 fusion.65
  20.7 1.9 %fusion.64 = (bf16[384,4096]{1,0:T(8,128)(2,1)}, bf16[384,4096]{1,0:T(8,128)(2,1)}) fusion(bf16[384,4096]{1,0:T(8,128)(2,1)} %get-tuple-element.64, bf16[2,32,4096]{2,1,0:T(8,128)(2,1)} %collective-permute-done.2, bf16[384,4096]{1,0:T(8,128)(2,1)} %get-tuple-element.65), kind=kLoop, calls=%fused_computation.99 | loop fusion | bytes 1048576
  22.5 0.8 fusion.63
  23.4 1.8 %fusion.62 = (bf16[384,4096]{1,0:T(8,128)(2,1)}, bf16[384,4096]{1,0:T(8,128)(2,1)}) fusion(bf16[384,4096]{1,0:T(8,128)(2,1)} %get-tuple-element.60, bf16[2,32,4096]{2,1,0:T(8,128)(2,1)} %collective-permute-done.3, bf16[384,4096]{1,0:T(8,128)(2,1)} %get-tuple-element.61), kind=kLoop, calls=%fused_computation.95 | loop fusion | bytes 1048576
  25.2 0.8 fusion.61
  26.0 1.8 %fusion.60 = (bf16[384,4096]{1,0:T(8,128)(2,1)}, bf16[384,4096]{1,0:T(8,128)(2,1)}) fusion(bf16[384,4096]{1,0:T(8,128)(2,1)} %get-tuple-element.56, bf16[2,32,4096]{2,1,0:T(8,128)(2,1)} %collective-permute-done.4, bf16[384,4096]{1,0:T(8,128)(2,1)} %get-tuple-element.57), kind=kLoop, calls=%fused_computation.91 | loop fusion | bytes 1048576
  27.9 0.8 fusion.59
  28.7 1.8 %fusion.58 = (bf16[384,4096]{1,0:T(8,128)(2,1)}, bf16[384,4096]{1,0:T(8,128)(2,1)}) fusion(bf16[384,4096]{1,0:T(8,128)(2,1)} %get-tuple-element.52, bf16[2,32,4096]{2,1,0:T(8,128)(2,1)} %collective-permute-done.5, bf16[384,4096]{1,0:T(8,128)(2,1)} %get-tuple-element.53), kind=kLoop, calls=%fused_computation.87 | loop fusion | bytes 1048576
  30.6 0.8 fusion.57
  31.4 0.8 fusion.56
  32.2 3.6 %all-to-all-done = bf16[64,32,256]{2,1,0:T(8,128)(2,1)S(1)} async-done(((bf16[64,32,256]{2,1,0:T(8,128)(2,1)}), bf16[64,32,256]{2,1,0:T(8,128)(2,1)S(1)}, u32[]{:S(2)}, u32[]{:S(2)}) %all-to-all-start) | async-done | bytes 1048608 | tf_op jit(solution)/shard_map/all_to_all | solution.py:19
  35.9 0.3 convert_element_type.85
  36.1 1.2 copy.124
  37.3 1.6 copy.187
  39.0 0.3 multiply_reduce_fusion
  39.5 3.6 %convolution_convert_fusion.1 = bf16[128,384]{1,0:T(8,128)(2,1)} fusion(bf16[384,4096]{1,0:T(8,128)(2,1)} %get-tuple-element.46, f32[128,4096]{1,0:T(8,128)S(1)} %bitcast.281, f32[4096]{0:T(1024)S(1)} %bitcast.320, f32[128]{0:T(128)S(1)} %rsqrt.36), kind=kOutput, calls=%fused_computation.45 | convolution fusion | flops 404275200 | bytes 5358080 | tf_op jit(solution)/shard_map/dot_general | solution.py:66
  43.1 3.5 %all-to-all-start.1 = ((bf16[4,32,384]{2,1,0:T(8,128)(2,1)}), bf16[4,32,384]{2,1,0:T(8,128)(2,1)S(1)}, u32[]{:S(2)}, u32[]{:S(2)}) async-start(bf16[4,32,384]{2,1,0:T(8,128)(2,1)} %bitcast.29), calls=%async_computation.1 | async-start | bytes 196608 | tf_op jit(solution)/shard_map/all_to_all | solution.py:69
  46.8 4.2 %all-to-all-done.1 = bf16[4,32,384]{2,1,0:T(8,128)(2,1)S(1)} async-done(((bf16[4,32,384]{2,1,0:T(8,128)(2,1)}), bf16[4,32,384]{2,1,0:T(8,128)(2,1)S(1)}, u32[]{:S(2)}, u32[]{:S(2)}) %all-to-all-start.1) | async-done | bytes 98336 | tf_op jit(solution)/shard_map/all_to_all | solution.py:69
  51.0 0.7 reshape.216
  51.7 0.8 fusion.107
  52.7 0.2 multiply_reduce_fusion.4
  53.6 3.4 %fusion = f32[32,4,1,64]{3,2,1,0:T(1,128)S(1)} fusion(f32[32,4,64,1]{2,3,1,0:T(1,128)S(1)} %bitcast.315, f32[2,32,4,64,64]{4,3,2,1,0:T(8,128)} %param.27), kind=kOutput, calls=%fused_computation.2 | convolution fusion | flops 1048576 | bytes 2162688 | tf_op jit(solution)/shard_map/bhij,bhj->bhi/dot_general | solution.py:31
  57.0 0.2 fusion.72
  57.2 4.2 %fusion.4 = f32[32,4,1,64]{3,2,1,0:T(1,128)S(1)} fusion(f32[32,4,64,1]{2,3,1,0:T(1,128)S(1)} %bitcast.322, f32[2,32,4,64,64]{4,3,2,1,0:T(8,128)} %param.27, f32[32,4,64]{2,1,0:T(4,128)S(1)} %bitcast_multiply_fusion.6, f32[32,4,64]{2,1,0:T(4,128)S(1)} %maximum_bitcast_fusion.1, f32[32,4,64]{2,1,0:T(4,128)S(1)} %get-tuple-element.12, ...), kind=kOutput, calls=%fused_computation.7 | convolution fusion | flops 4194304 | bytes 4423712 | tf_op jit(solution)/shard_map/bhij,bhj->bhi/dot_general | solution.py:38
  61.7 0.2 fusion.99
  62.0 1.1 broadcast_in_dim.43
  63.1 5.2 %all-to-all-start.2 = ((bf16[64,32,256]{2,1,0:T(8,128)(2,1)}), bf16[64,32,256]{2,1,0:T(8,128)(2,1)S(1)}, u32[]{:S(2)}, u32[]{:S(2)}) async-start(bf16[64,32,256]{2,1,0:T(8,128)(2,1)} %broadcast_in_dim.43), calls=%async_computation.2 | async-start | bytes 2097152 | tf_op jit(solution)/shard_map/all_to_all | solution.py:19
  68.5 1.1 slice_bitcast_fusion.26
  69.5 15.2 %all-to-all-done.2 = bf16[64,32,256]{2,1,0:T(8,128)(2,1)S(1)} async-done(((bf16[64,32,256]{2,1,0:T(8,128)(2,1)}), bf16[64,32,256]{2,1,0:T(8,128)(2,1)S(1)}, u32[]{:S(2)}, u32[]{:S(2)}) %all-to-all-start.2) | async-done | bytes 1048608 | tf_op jit(solution)/shard_map/all_to_all | solution.py:19
  84.8 0.6 copy.138
  85.4 0.4 copy.188
  85.8 0.5 convolution_convert_fusion.3
  86.3 0.2 broadcast_in_dim.44
  86.6 24.6 %all_to_all.35 = bf16[64,64,128]{2,1,0:T(8,128)(2,1)S(1)} all-to-all(bf16[64,64,128]{2,1,0:T(8,128)(2,1)S(1)} %broadcast_in_dim.44), channel_id=1, replica_groups=mesh['z'=4,'y'=4,'x'=4,'c'=2] {'z','y','x'}, dimensions={0} | all-to-all | bytes 2097152 | tf_op jit(solution)/shard_map/all_to_all | solution.py:19
  111.2 0.6 fusion.18
  111.8 2.5 %convolution_convert_fusion = bf16[128,384]{1,0:T(8,128)(2,1)} fusion(bf16[384,4096]{1,0:T(8,128)(2,1)S(1)} %copy-done.8, bf16[4096,128]{1,0:T(8,128)(2,1)S(1)} %bitcast.286, f32[4096]{0:T(1024)S(1)} %bitcast.323, f32[128]{0:T(128)S(1)} %add_rsqrt_fusion.3), kind=kOutput, calls=%fused_computation.44 | convolution fusion | flops 404799488 | bytes 4309504 | tf_op jit(solution)/shard_map/dot_general | solution.py:66
  114.4 3.5 %all-to-all-start.4 = ((bf16[4,32,384]{2,1,0:T(8,128)(2,1)}), bf16[4,32,384]{2,1,0:T(8,128)(2,1)S(1)}, u32[]{:S(2)}, u32[]{:S(2)}) async-start(bf16[4,32,384]{2,1,0:T(8,128)(2,1)} %bitcast.73), calls=%async_computation.4 | async-start | bytes 196608 | tf_op jit(solution)/shard_map/all_to_all | solution.py:69
  118.2 4.2 %all-to-all-done.4 = bf16[4,32,384]{2,1,0:T(8,128)(2,1)S(1)} async-done(((bf16[4,32,384]{2,1,0:T(8,128)(2,1)}), bf16[4,32,384]{2,1,0:T(8,128)(2,1)S(1)}, u32[]{:S(2)}, u32[]{:S(2)}) %all-to-all-start.4) | async-done | bytes 98336 | tf_op jit(solution)/shard_map/all_to_all | solution.py:69
  122.3 0.7 reshape.218
  123.0 0.8 fusion.106
  123.8 0.2 multiply_reduce_fusion.2
  124.3 3.4 %fusion.5 = f32[32,4,1,64]{3,2,1,0:T(1,128)S(1)} fusion(f32[32,4,64,1]{2,3,1,0:T(1,128)S(1)} %bitcast.316, f32[2,32,4,64,64]{4,3,2,1,0:T(8,128)} %param.27), kind=kOutput, calls=%fused_computation.9 | convolution fusion | flops 1048576 | bytes 2162688 | tf_op jit(solution)/shard_map/bhij,bhj->bhi/dot_general | solution.py:31
  128.2 0.2 fusion.77
  128.4 4.2 %fusion.9 = f32[32,4,1,64]{3,2,1,0:T(1,128)S(1)} fusion(f32[32,4,64,1]{2,3,1,0:T(1,128)S(1)} %bitcast.321, f32[2,32,4,64,64]{4,3,2,1,0:T(8,128)} %param.27, f32[32,4,64]{2,1,0:T(4,128)S(1)} %bitcast_multiply_fusion.3, f32[32,4,64]{2,1,0:T(4,128)S(1)} %maximum_bitcast_fusion.3, f32[32,4,64]{2,1,0:T(4,128)S(1)} %get-tuple-element.8, ...), kind=kOutput, calls=%fused_computation.14 | convolution fusion | flops 4194304 | bytes 4423712 | tf_op jit(solution)/shard_map/bhij,bhj->bhi/dot_general | solution.py:38
  133.0 0.2 fusion.97
  133.3 1.1 broadcast_in_dim.46
  134.4 6.5 %all-to-all-start.5 = ((bf16[64,32,256]{2,1,0:T(8,128)(2,1)}), bf16[64,32,256]{2,1,0:T(8,128)(2,1)S(1)}, u32[]{:S(2)}, u32[]{:S(2)}) async-start(bf16[64,32,256]{2,1,0:T(8,128)(2,1)} %broadcast_in_dim.46), calls=%async_computation.5 | async-start | bytes 2097152 | tf_op jit(solution)/shard_map/all_to_all | solution.py:19
  140.9 10.7 %add_select_fusion.1 = (f32[1,32,4,64,64]{4,3,2,1,0:T(8,128)}, f32[1,32,4,64,64]{4,3,2,1,0:T(8,128)}) fusion(f32[2,32,4,64,64]{4,3,2,1,0:T(8,128)} %param.27, f32[32,4,64]{2,1,0:T(4,128)S(1)} %bitcast_multiply_fusion.6, f32[32,4,64]{2,1,0:T(4,128)S(1)} %maximum_bitcast_fusion.1, f32[32,4,64]{2,1,0:T(4,128)S(1)} %get-tuple-element.12, ...), kind=kLoop, calls=%fused_computation.16 | loop fusion | flops 6291456 | bytes 8716320 | tf_op jit(solution)/shard_map/jit(_where)/select_n | solution.py:37
  151.6 8.8 %all-to-all-done.5 = bf16[64,32,256]{2,1,0:T(8,128)(2,1)S(1)} async-done(((bf16[64,32,256]{2,1,0:T(8,128)(2,1)}), bf16[64,32,256]{2,1,0:T(8,128)(2,1)S(1)}, u32[]{:S(2)}, u32[]{:S(2)}) %all-to-all-start.5) | async-done | bytes 1048608 | tf_op jit(solution)/shard_map/all_to_all | solution.py:19
  160.4 0.6 copy.151
  161.0 0.4 copy.189
  161.4 0.5 convolution_convert_fusion.2
  162.1 0.7 reshape.260
  162.8 3.3 %all-to-all-start.6 = ((bf16[4,2,1024]{2,1,0:T(2,128)(2,1)}), bf16[4,2,1024]{2,1,0:T(2,128)(2,1)S(1)}, u32[]{:S(2)}, u32[]{:S(2)}) async-start(bf16[4,2,1024]{2,1,0:T(2,128)(2,1)} %reshape.260), calls=%async_computation.6 | async-start | bytes 32768 | tf_op jit(solution)/shard_map/all_to_all | solution.py:106
  166.1 8.8 %pad_maximum_fusion = f32[2,32,4,64,64]{4,3,2,1,0:T(8,128)} fusion(f32[1,32,4,64,64]{4,3,2,1,0:T(8,128)} %get-tuple-element.17, f32[1,32,4,64,64]{4,3,2,1,0:T(8,128)} %get-tuple-element.16), kind=kLoop, calls=%fused_computation | loop fusion | flops 1048576 | bytes 8388608 | tf_op jit(solution)/shard_map/stack | solution.py:108
  174.9 0.7 reshape.214
  (88 shorter events, 4.0 us)
Async XLA Ops:
  0.6 15.8 %copy-start = (bf16[2,4096,32]{1,2,0:T(8,128)(2,1)S(1)}, bf16[2,4096,32]{1,2,0:T(8,128)(2,1)}, u32[]{:S(2)}) copy-start(bf16[2,4096,32]{1,2,0:T(8,128)(2,1)} %param.17) | copy-start | bytes 1572868
  0.6 19.1 %copy-start.1 = (bf16[2,4096,32]{1,2,0:T(8,128)(2,1)S(1)}, bf16[2,4096,32]{1,2,0:T(8,128)(2,1)}, u32[]{:S(2)}) copy-start(bf16[2,4096,32]{1,2,0:T(8,128)(2,1)} %param.18) | copy-start | bytes 1572868
  0.7 16.6 %copy-start.7 = (f32[2,4096]{1,0:T(2,128)S(1)}, f32[2,4096]{1,0:T(2,128)}, u32[]{:S(2)}) copy-start(f32[2,4096]{1,0:T(2,128)} %param.16) | copy-start | bytes 98308
  0.7 16.6 %copy-start.10 = (f32[2,256]{1,0:T(2,128)S(1)}, f32[2,256]{1,0:T(2,128)}, u32[]{:S(2)}) copy-start(f32[2,256]{1,0:T(2,128)} %param.26) | copy-start | bytes 6148
  0.7 16.6 %copy-start.11 = (f32[2,256]{1,0:T(2,128)S(1)}, f32[2,256]{1,0:T(2,128)}, u32[]{:S(2)}) copy-start(f32[2,256]{1,0:T(2,128)} %param.25) | copy-start | bytes 6148
  0.7 16.7 %copy-start.12 = (s32[32]{0:T(128)S(1)}, s32[32]{0:T(128)}, u32[]{:S(2)}) copy-start(s32[32]{0:T(128)} %param.15) | copy-start | bytes 388
  0.7 16.7 %collective-permute-start.1 = (bf16[2,32,4096]{2,1,0:T(8,128)(2,1)}, bf16[2,32,4096]{2,1,0:T(8,128)(2,1)}, u32[]{:S(2)}, u32[]{:S(2)}) collective-permute-start(bf16[2,32,4096]{2,1,0:T(8,128)(2,1)} %bitcast.297), channel_id=1, source_target_pairs={{0,1},{1,0},{2,3},{3,2},{4,5},{5,4},{6,7},{7,6},{8,9},{9,8},{10,11... | collective-permute-start | bytes 1572872 | tf_op jit(solution)/shard_map/ppermute | solution.py:57
  2.1 18.4 %collective-permute-start.2 = (bf16[2,32,4096]{2,1,0:T(8,128)(2,1)}, bf16[2,32,4096]{2,1,0:T(8,128)(2,1)}, u32[]{:S(2)}, u32[]{:S(2)}) collective-permute-start(bf16[2,32,4096]{2,1,0:T(8,128)(2,1)} %bitcast.299), channel_id=1, source_target_pairs={{0,1},{1,0},{2,3},{3,2},{4,5},{5,4},{6,7},{7,6},{8,9},{9,8},{10,11... | collective-permute-start | bytes 1572872 | tf_op jit(solution)/shard_map/ppermute | solution.py:57
  2.2 21.1 %collective-permute-start.3 = (bf16[2,32,4096]{2,1,0:T(8,128)(2,1)}, bf16[2,32,4096]{2,1,0:T(8,128)(2,1)}, u32[]{:S(2)}, u32[]{:S(2)}) collective-permute-start(bf16[2,32,4096]{2,1,0:T(8,128)(2,1)} %bitcast.301), channel_id=1, source_target_pairs={{0,1},{1,0},{2,3},{3,2},{4,5},{5,4},{6,7},{7,6},{8,9},{9,8},{10,11... | collective-permute-start | bytes 1572872 | tf_op jit(solution)/shard_map/ppermute | solution.py:57
  2.6 23.4 %collective-permute-start.4 = (bf16[2,32,4096]{2,1,0:T(8,128)(2,1)}, bf16[2,32,4096]{2,1,0:T(8,128)(2,1)}, u32[]{:S(2)}, u32[]{:S(2)}) collective-permute-start(bf16[2,32,4096]{2,1,0:T(8,128)(2,1)} %bitcast.303), channel_id=1, source_target_pairs={{0,1},{1,0},{2,3},{3,2},{4,5},{5,4},{6,7},{7,6},{8,9},{9,8},{10,11... | collective-permute-start | bytes 1572872 | tf_op jit(solution)/shard_map/ppermute | solution.py:57
  2.7 26.0 %collective-permute-start.5 = (bf16[2,32,4096]{2,1,0:T(8,128)(2,1)}, bf16[2,32,4096]{2,1,0:T(8,128)(2,1)}, u32[]{:S(2)}, u32[]{:S(2)}) collective-permute-start(bf16[2,32,4096]{2,1,0:T(8,128)(2,1)} %bitcast.305), channel_id=1, source_target_pairs={{0,1},{1,0},{2,3},{3,2},{4,5},{5,4},{6,7},{7,6},{8,9},{9,8},{10,11... | collective-permute-start | bytes 1572872 | tf_op jit(solution)/shard_map/ppermute | solution.py:57
  5.0 17.6 %copy-start.2 = (bf16[2,4096,32]{1,2,0:T(8,128)(2,1)S(1)}, bf16[2,4096,32]{1,2,0:T(8,128)(2,1)}, u32[]{:S(2)}) copy-start(bf16[2,4096,32]{1,2,0:T(8,128)(2,1)} %param.19) | copy-start | bytes 1572868
  5.0 30.9 %all-to-all-start = ((bf16[64,32,256]{2,1,0:T(8,128)(2,1)}), bf16[64,32,256]{2,1,0:T(8,128)(2,1)S(1)}, u32[]{:S(2)}, u32[]{:S(2)}) async-start(bf16[64,32,256]{2,1,0:T(8,128)(2,1)} %broadcast_in_dim.41), calls=%async_computation | async-start | bytes 2097152 | tf_op jit(solution)/shard_map/all_to_all | solution.py:19
  16.4 8.8 %copy-start.3 = (bf16[2,4096,32]{1,2,0:T(8,128)(2,1)S(1)}, bf16[2,4096,32]{1,2,0:T(8,128)(2,1)}, u32[]{:S(2)}) copy-start(bf16[2,4096,32]{1,2,0:T(8,128)(2,1)} %param.20) | copy-start | bytes 1572868
  17.4 14.0 %collective-permute-start.6 = (bf16[2,32,4096]{2,1,0:T(8,128)(2,1)}, bf16[2,32,4096]{2,1,0:T(8,128)(2,1)S(1)}, u32[]{:S(2)}, u32[]{:S(2)}) collective-permute-start(bf16[2,32,4096]{2,1,0:T(8,128)(2,1)} %bitcast.307), channel_id=1, source_target_pairs={{0,1},{1,0},{2,3},{3,2},{4,5},{5,4},{6,7},{7,6},{8,9},{9,8},{10,11... | collective-permute-start | bytes 1572872 | tf_op jit(solution)/shard_map/ppermute | solution.py:57
  19.7 8.2 %copy-start.4 = (bf16[2,4096,32]{1,2,0:T(8,128)(2,1)S(1)}, bf16[2,4096,32]{1,2,0:T(8,128)(2,1)}, u32[]{:S(2)}) copy-start(bf16[2,4096,32]{1,2,0:T(8,128)(2,1)} %param.21) | copy-start | bytes 1572868
  20.5 47.9 %collective-permute-start = (bf16[2,32,4096]{2,1,0:T(8,128)(2,1)}, bf16[2,32,4096]{2,1,0:T(8,128)(2,1)}, u32[]{:S(2)}, u32[]{:S(2)}) collective-permute-start(bf16[2,32,4096]{2,1,0:T(8,128)(2,1)} %bitcast.309), channel_id=1, source_target_pairs={{0,1},{1,0},{2,3},{3,2},{4,5},{5,4},{6,7},{7,6},{8,9},{9,8},{10,11... | collective-permute-start | bytes 1572872 | tf_op jit(solution)/shard_map/ppermute | solution.py:57
  22.5 8.0 %copy-start.5 = (bf16[2,4096,32]{1,2,0:T(8,128)(2,1)S(1)}, bf16[2,4096,32]{1,2,0:T(8,128)(2,1)}, u32[]{:S(2)}) copy-start(bf16[2,4096,32]{1,2,0:T(8,128)(2,1)} %param.22) | copy-start | bytes 1572868
  39.0 7.6 %copy-start.9 = (f32[2,256]{1,0:T(2,128)S(1)}, f32[2,256]{1,0:T(2,128)}, u32[]{:S(2)}) copy-start(f32[2,256]{1,0:T(2,128)} %param.24) | copy-start | bytes 6148
  43.1 7.9 %all-to-all-start.1 = ((bf16[4,32,384]{2,1,0:T(8,128)(2,1)}), bf16[4,32,384]{2,1,0:T(8,128)(2,1)S(1)}, u32[]{:S(2)}, u32[]{:S(2)}) async-start(bf16[4,32,384]{2,1,0:T(8,128)(2,1)} %bitcast.29), calls=%async_computation.1 | async-start | bytes 196608 | tf_op jit(solution)/shard_map/all_to_all | solution.py:69
  61.4 7.0 %copy-start.6 = (bf16[2,4096,32]{1,2,0:T(8,128)(2,1)S(1)}, bf16[2,4096,32]{1,2,0:T(8,128)(2,1)}, u32[]{:S(2)}) copy-start(bf16[2,4096,32]{1,2,0:T(8,128)(2,1)} %param.23) | copy-start | bytes 1572868
  63.1 21.6 %all-to-all-start.2 = ((bf16[64,32,256]{2,1,0:T(8,128)(2,1)}), bf16[64,32,256]{2,1,0:T(8,128)(2,1)S(1)}, u32[]{:S(2)}, u32[]{:S(2)}) async-start(bf16[64,32,256]{2,1,0:T(8,128)(2,1)} %broadcast_in_dim.43), calls=%async_computation.2 | async-start | bytes 2097152 | tf_op jit(solution)/shard_map/all_to_all | solution.py:19
  85.8 26.1 %copy-start.8 = (bf16[384,4096]{1,0:T(8,128)(2,1)S(1)}, bf16[384,4096]{1,0:T(8,128)(2,1)}, u32[]{:S(2)}) copy-start(bf16[384,4096]{1,0:T(8,128)(2,1)} %get-tuple-element.47) | copy-start | bytes 9437188
  114.4 7.9 %all-to-all-start.4 = ((bf16[4,32,384]{2,1,0:T(8,128)(2,1)}), bf16[4,32,384]{2,1,0:T(8,128)(2,1)S(1)}, u32[]{:S(2)}, u32[]{:S(2)}) async-start(bf16[4,32,384]{2,1,0:T(8,128)(2,1)} %bitcast.73), calls=%async_computation.4 | async-start | bytes 196608 | tf_op jit(solution)/shard_map/all_to_all | solution.py:69
  134.4 26.0 %all-to-all-start.5 = ((bf16[64,32,256]{2,1,0:T(8,128)(2,1)}), bf16[64,32,256]{2,1,0:T(8,128)(2,1)S(1)}, u32[]{:S(2)}, u32[]{:S(2)}) async-start(bf16[64,32,256]{2,1,0:T(8,128)(2,1)} %broadcast_in_dim.46), calls=%async_computation.5 | async-start | bytes 2097152 | tf_op jit(solution)/shard_map/all_to_all | solution.py:19
  162.8 12.0 %all-to-all-start.6 = ((bf16[4,2,1024]{2,1,0:T(2,128)(2,1)}), bf16[4,2,1024]{2,1,0:T(2,128)(2,1)S(1)}, u32[]{:S(2)}, u32[]{:S(2)}) async-start(bf16[4,2,1024]{2,1,0:T(2,128)(2,1)} %reshape.260), calls=%async_computation.6 | async-start | bytes 32768 | tf_op jit(solution)/shard_map/all_to_all | solution.py:106
